TPU v7x, 768 devices: a whole 4x8x12 slice. The times are simulated.
768 devices in a mesh: rep: 3 (over z_hi), fs: 32 (over z_lo, y), tp: 8 (over x, core).
Axes of the slice: x: 4, y: 8, z: 12 (z_hi: 3, z_lo: 4; z = z_hi * 4 + z_lo), core: 2. Of those that a mesh axis runs over, the one named last changes fastest.
Arguments:
- tokens: bfloat16 [24576, 2048], P(('rep', 'fs')), may hold values from -6 to 6
- mix_gain: float32 [2048], replicated, may hold values from 0.1 to 1.9
- group_weight: float32 [512, 2048], P('fs', 'tp'), may hold values from -0.25 to 0.25
- group_scale: float32 [1, 2048], P(None, 'tp'), may hold values from 0.5 to 2
- mlp_gain: float32 [2048], replicated, may hold values from 0.1 to 1.9
- up_weight: float32 [2048, 8192], P('fs', 'tp'), may hold values from -0.125 to 0.125
- up_scale: float32 [1, 8192], P(None, 'tp'), may hold values from 0.5 to 2
- down_weight: float32 [8192, 2048], P('tp', 'fs'), may hold values from -0.0625 to 0.0625
- down_scale: float32 [1, 2048], replicated, may hold values from 0.5 to 2
Outputs:
- layer_out: bfloat16 [24576, 2048], P(('rep', 'fs'))
All inputs are finite; a program needn't handle non-finite values.
Results may differ from a plain program's by a relative error of at most 0.013.
Values may be sent and summed in bfloat16 or wider, within the bound.
A program may use at most 64 MiB of HBM per device.

v0:
```python
import jax
import jax.numpy as jnp
from jax import lax
from jax.sharding import Mesh
from jax.sharding import PartitionSpec as P

GROUPS = 4
LENGTH = 128
FS = ("fs_0", "fs_1")
REP_FS = ("rep", "fs_0", "fs_1")


norm_eps = 1e-06


def in_order(parts, dim):
    shape = list(parts.shape[1:])
    shape[dim] *= parts.shape[0]
    return jnp.moveaxis(parts, 0, dim).reshape(shape)


def stacked_from(value, axes, sequence):
    parts = value
    for k in sequence:
        parts = lax.all_gather(parts, axes[k])
    done = sequence[::-1]
    back = [done.index(k) for k in range(len(axes))]
    parts = parts.transpose(*back, *range(len(axes), parts.ndim))
    return parts.reshape(-1, *value.shape)


def gather_axes(value, axes, sequence, dim):
    return in_order(stacked_from(value, axes, sequence), dim)


def copy_for_each(value, axis):
    length = lax.axis_size(axis)
    return lax.all_to_all(
        jnp.broadcast_to(value[None], (length, *value.shape)), axis, 0, 0, tiled=True
    )


def collect(value, axis, dim):
    parts = copy_for_each(value, axis)
    return in_order(parts, dim)


def total_of_pieces(value, axis):
    parts = lax.all_gather(value, axis).astype(jnp.float32)
    return parts.sum(axis=0)


def norm_rows(values, gain):
    promoted = values.astype(jnp.float32)
    inverse = lax.rsqrt(jnp.mean(promoted * promoted, axis=-1, keepdims=True) + norm_eps)
    return (promoted * inverse * gain).astype(jnp.bfloat16)


def band_means(inputs, window, seq_length):
    row_count, columns = inputs.shape
    by_sequence = inputs.reshape(row_count // seq_length, seq_length, columns)
    position = jnp.arange(seq_length, dtype=jnp.int32)
    offset = position[:, None] - position[None, :]
    band_mask = ((offset >= 0) & (offset < window)).astype(jnp.bfloat16)
    divisor = jnp.minimum(position + 1, window).astype(jnp.float32)
    summed = jnp.einsum("ts,nsc->ntc", band_mask, by_sequence, preferred_element_type=jnp.float32)
    return (summed / divisor[None, :, None] - by_sequence.astype(jnp.float32)).reshape(
        row_count, columns
    )


def body(
    tokens,
    mix_gain,
    group_weight,
    group_scale,
    mlp_gain,
    up_weight,
    up_scale,
    down_weight,
    down_scale,
):
    up_whole = gather_axes(up_weight.astype(jnp.bfloat16), FS, (0, 1), 0)
    down_whole = gather_axes(down_weight.astype(jnp.bfloat16), FS, (0, 1), 1)
    model_width = tokens.shape[1]
    group_width = model_width // GROUPS
    own_cols = group_weight.shape[1]
    column_start = lax.axis_index("tp") * own_cols
    group_index = column_start // group_width
    normed = norm_rows(tokens, mix_gain)
    inputs = lax.dynamic_slice_in_dim(normed, group_index * group_width, group_width, 1)
    window = jnp.left_shift(jnp.int32(2), group_index)
    pooled = band_means(inputs, window, LENGTH).astype(jnp.bfloat16)
    mixed_cols = (
        jnp.dot(
            pooled,
            collect(group_weight.astype(jnp.bfloat16), FS, 0),
            preferred_element_type=jnp.float32,
        )
        * group_scale
    )
    own_tokens = lax.dynamic_slice_in_dim(tokens, column_start, own_cols, 1)
    carried_cols = (own_tokens.astype(jnp.float32) + mixed_cols).astype(jnp.bfloat16)
    carried = collect(carried_cols, "tp", 1)
    normed_mlp = norm_rows(carried, mlp_gain)
    pre_act = jnp.dot(normed_mlp, up_whole, preferred_element_type=jnp.float32) * up_scale
    hidden = jnp.square(jax.nn.relu(pre_act)).astype(jnp.bfloat16)
    partial_value = jnp.dot(hidden, down_whole, preferred_element_type=jnp.float32) * down_scale
    summed = total_of_pieces(partial_value.astype(jnp.bfloat16), "tp").astype(jnp.float32)
    return (carried.astype(jnp.float32) + summed).astype(jnp.bfloat16)


def solution(mesh):
    split = Mesh(
        mesh.devices.reshape(mesh.shape["rep"], 4, 8, mesh.shape["tp"]),
        ("rep", "fs_0", "fs_1", "tp"),
    )
    return jax.shard_map(
        body,
        mesh=split,
        in_specs=(
            P(REP_FS, None),
            P(),
            P(FS, "tp"),
            P(None, "tp"),
            P(),
            P(FS, "tp"),
            P(None, "tp"),
            P("tp", FS),
            P(),
        ),
        out_specs=P(REP_FS, None),
        check_vma=False,
    )
```

profile of v0, /device:TPU:1, one launch (start us, length us, event | category | flops | bytes accessed | tf_op | source)
XLA Modules:
  0.0 241.5 jit_solution(762163327462687328)
XLA Ops:
  6.5 0.0 copy-start.1
  6.5 0.0 copy-start.2
  6.5 0.0 all-gather.11.cloned.1.call-start
  6.5 1.0 convert_element_type.85
  7.6 15.4 %all-gather.2 = bf16[4096,64]{0,1:T(8,128)(2,1)S(1)} all-gather(bf16[1024,64]{0,1:T(8,128)(2,1)S(1)} %convert_element_type.85), channel_id=4, replica_groups=mesh['rep'=3,'fs_0'=4,'fs_1'=8,'tp'=8] {'fs_0'}, dimensions={0}, use_global_device_ids=true | all-gather | bytes 655360 | tf_op jit(solution)/shard_map/all_gather | solution.py:25
  23.0 0.0 copy-start
  23.0 0.9 copy.30
  23.8 0.0 all-gather.11.cloned.1.call-update
  23.9 0.0 all-gather.9.cloned.1.call-start
  23.9 0.0 copy-done.1
  23.9 12.8 %all-gather = bf16[256,1024]{1,0:T(8,128)(2,1)} all-gather(bf16[64,1024]{1,0:T(8,128)(2,1)S(1)} %convert_element_type.83), channel_id=2, replica_groups=mesh['rep'=3,'fs_0'=4,'fs_1'=8,'tp'=8] {'fs_0'}, dimensions={0}, use_global_device_ids=true | all-gather | bytes 655360 | tf_op jit(solution)/shard_map/all_gather | solution.py:25
  36.8 0.0 all-gather.9.cloned.1.call-update
  36.8 0.0 copy-done.2
  36.8 0.7 broadcast_in_dim.4
  37.5 12.8 %all-to-all-start = ((bf16[32,16,256]{2,1,0:T(8,128)(2,1)}), bf16[32,16,256]{2,1,0:T(8,128)(2,1)S(1)}, u32[]{:S(2)}, u32[]{:S(2)}) async-start(bf16[32,16,256]{2,1,0:T(8,128)(2,1)} %broadcast_in_dim.4), calls=%async_computation | async-start | bytes 524288 | tf_op jit(solution)/shard_map/all_to_all | solution.py:38
  50.3 0.0 copy-done
  50.3 0.2 convert_element_type.70
  50.6 0.0 copy-start.4
  50.6 0.8 dynamic-slice
  51.4 0.3 multiply_reduce_fusion.1
  51.7 0.1 fusion.10
  51.8 0.2 fusion.6
  52.0 0.0 copy-start.3
  52.0 8.4 %all-to-all-done = bf16[32,16,256]{2,1,0:T(8,128)(2,1)S(1)} async-done(((bf16[32,16,256]{2,1,0:T(8,128)(2,1)}), bf16[32,16,256]{2,1,0:T(8,128)(2,1)S(1)}, u32[]{:S(2)}, u32[]{:S(2)}) %all-to-all-start) | async-done | bytes 262176 | tf_op jit(solution)/shard_map/all_to_all | solution.py:38
  60.4 0.0 copy-done.4
  60.4 0.2 fusion.8
  60.6 1.0 broadcast_in_dim.5
  61.7 10.9 %all-to-all-start.1 = ((bf16[8,256,256]{2,1,0:T(8,128)(2,1)}), bf16[8,256,256]{2,1,0:T(8,128)(2,1)S(1)}, u32[]{:S(2)}, u32[]{:S(2)}) async-start(bf16[8,256,256]{2,1,0:T(8,128)(2,1)} %broadcast_in_dim.5), calls=%async_computation.1 | async-start | bytes 2097152 | tf_op jit(solution)/shard_map/all_to_all | solution.py:38
  72.6 0.0 all-gather.13.cloned.1.call-start
  72.6 0.0 copy-done.3
  72.6 14.9 %all-to-all-done.1 = bf16[8,256,256]{2,1,0:T(8,128)(2,1)S(1)} async-done(((bf16[8,256,256]{2,1,0:T(8,128)(2,1)}), bf16[8,256,256]{2,1,0:T(8,128)(2,1)S(1)}, u32[]{:S(2)}, u32[]{:S(2)}) %all-to-all-start.1) | async-done | bytes 1048608 | tf_op jit(solution)/shard_map/all_to_all | solution.py:38
  87.5 0.5 copy.23
  88.1 0.3 multiply_reduce_fusion
  88.4 0.3 multiply_convert_fusion
  88.7 9.1 %all-gather.11.cloned.1.call-done = bf16[32,1024,64]{1,2,0:T(8,128)(2,1)} async-done(((bf16[4,1024,64]{1,2,0:T(8,128)(2,1)}), bf16[32,1024,64]{1,2,0:T(8,128)(2,1)}) %all-gather.11.cloned.1.call-update) | async-done | bytes 4194320 | tf_op jit(solution)/shard_map/all_gather | solution.py:25
  97.8 4.9 %copy.26 = bf16[4,8,1024,64]{2,3,1,0:T(8,128)(2,1)} copy(bf16[4,8,1024,64]{2,3,0,1:T(8,128)(2,1)} %bitcast.48) | data formatting | bytes 8388608 | tf_op jit(solution)/shard_map/transpose | solution.py:28
  102.7 56.4 %all-gather.9.cloned.1.call-done = bf16[32,64,1024]{2,1,0:T(8,128)(2,1)} async-done(((bf16[4,64,1024]{2,1,0:T(8,128)(2,1)}), bf16[32,64,1024]{2,1,0:T(8,128)(2,1)}) %all-gather.9.cloned.1.call-update) | async-done | bytes 4194320 | tf_op jit(solution)/shard_map/all_gather | solution.py:25
  159.1 0.0 copy-start.5
  159.1 4.9 %copy.24 = bf16[4,8,64,1024]{3,2,1,0:T(8,128)(2,1)} copy(bf16[4,8,64,1024]{3,2,0,1:T(8,128)(2,1)} %bitcast.49) | data formatting | bytes 8388608 | tf_op jit(solution)/shard_map/transpose | solution.py:28
  164.0 0.0 copy-done.5
  164.0 0.0 copy-done.6
  164.0 6.8 %fusion = bf16[256,2048]{1,0:T(8,128)(2,1)} fusion(bf16[1024,2048]{0,1:T(8,128)(2,1)} %bitcast.50, f32[2048]{0:T(1024)S(1)} %bitcast.60, bf16[256,2048]{0,1:T(8,128)(2,1)S(1)} %bitcast.56, bf16[2048,1024]{1,0:T(8,128)(2,1)} %bitcast.51, f32[1024]{0:T(1024)S(1)} %bitcast.61), kind=kOutput, calls=%fused_computation.2 | convolution fusion | flops 2149580800 | bytes 10498048 | tf_op jit(solution)/shard_map/dot_general | solution.py:108
  170.8 0.0 all-gather.13.cloned.1.call-update
  170.8 1.6 convert_element_type.90
  172.4 1.9 copy.27
  174.3 54.0 %all-gather.13.cloned.1.call-done = bf16[2048,2048]{1,0:T(8,128)(2,1)} async-done(((bf16[256,2048]{1,0:T(8,128)(2,1)}), bf16[2048,2048]{1,0:T(8,128)(2,1)}) %all-gather.13.cloned.1.call-update) | async-done | bytes 8388624 | tf_op jit(solution)/shard_map/all_gather | solution.py:49
  228.3 5.4 %convert_reduce_fusion = f32[256,2048]{1,0:T(8,128)S(1)} fusion(bf16[8,256,2048]{2,1,0:T(8,128)(2,1)} %bitcast.46), kind=kLoop, calls=%fused_computation | loop fusion | flops 7864320 | bytes 10485760 | tf_op jit(solution)/shard_map/reduce_sum | solution.py:50
  233.8 1.3 add_convert_fusion
  (7 shorter events, 0.0 us)
Async XLA Ops:
  6.5 17.4 %copy-start.1 = (f32[64,1024]{1,0:T(8,128)S(1)}, f32[64,1024]{1,0:T(8,128)}, u32[]{:S(2)}) copy-start(f32[64,1024]{1,0:T(8,128)} %param.14) | copy-start | bytes 786436
  6.5 30.3 %copy-start.2 = (f32[16,256]{1,0:T(8,128)S(1)}, f32[16,256]{1,0:T(8,128)}, u32[]{:S(2)}) copy-start(f32[16,256]{1,0:T(8,128)} %param.11) | copy-start | bytes 49156
  6.5 91.3 %all-gather.11.cloned.1.call-start = ((), (), s32[]{:S(2)}) async-start(), calls=%async_computation.3 | async-start | bytes 4718592 | tf_op jit(solution)/shard_map/all_gather | solution.py:25
  23.0 27.4 %copy-start = (bf16[256,2048]{1,0:T(8,128)(2,1)S(1)}, bf16[256,2048]{1,0:T(8,128)(2,1)}, u32[]{:S(2)}) copy-start(bf16[256,2048]{1,0:T(8,128)(2,1)} %param.9) | copy-start | bytes 3145732
  23.9 135.2 %all-gather.9.cloned.1.call-start = ((), (), s32[]{:S(2)}) async-start(), calls=%async_computation.2 | async-start | bytes 4718592 | tf_op jit(solution)/shard_map/all_gather | solution.py:25
  37.5 22.8 %all-to-all-start = ((bf16[32,16,256]{2,1,0:T(8,128)(2,1)}), bf16[32,16,256]{2,1,0:T(8,128)(2,1)S(1)}, u32[]{:S(2)}, u32[]{:S(2)}) async-start(bf16[32,16,256]{2,1,0:T(8,128)(2,1)} %broadcast_in_dim.4), calls=%async_computation | async-start | bytes 524288 | tf_op jit(solution)/shard_map/all_to_all | solution.py:38
  50.6 9.8 %copy-start.4 = (f32[1,256]{1,0:T(1,128)S(1)}, f32[1,256]{1,0:T(1,128)}, u32[]{:S(2)}) copy-start(f32[1,256]{1,0:T(1,128)} %param.12) | copy-start | bytes 3076
  52.0 20.6 %copy-start.3 = (f32[2048]{0:T(1024)S(1)}, f32[2048]{0:T(1024)}, u32[]{:S(2)}) copy-start(f32[2048]{0:T(1024)} %param.13) | copy-start | bytes 24580
  61.7 25.9 %all-to-all-start.1 = ((bf16[8,256,256]{2,1,0:T(8,128)(2,1)}), bf16[8,256,256]{2,1,0:T(8,128)(2,1)S(1)}, u32[]{:S(2)}, u32[]{:S(2)}) async-start(bf16[8,256,256]{2,1,0:T(8,128)(2,1)} %broadcast_in_dim.5), calls=%async_computation.1 | async-start | bytes 2097152 | tf_op jit(solution)/shard_map/all_to_all | solution.py:38
  72.6 155.8 %all-gather.13.cloned.1.call-start = ((), (), s32[]{:S(2)}) async-start(), calls=%async_computation.4 | async-start | bytes 9437184 | tf_op jit(solution)/shard_map/all_gather | solution.py:49
  159.1 4.9 %copy-start.5 = (f32[1,2048]{1,0:T(1,128)S(1)}, f32[1,2048]{1,0:T(1,128)}, u32[]{:S(2)}) copy-start(f32[1,2048]{1,0:T(1,128)} %param.17) | copy-start | bytes 24580
  159.1 4.9 %copy-start.6 = (f32[1,1024]{1,0:T(1,128)S(1)}, f32[1,1024]{1,0:T(1,128)}, u32[]{:S(2)}) copy-start(f32[1,1024]{1,0:T(1,128)} %param.15) | copy-start | bytes 12292
Sparse Core Ops, SparseCore 0:
  24.0 73.7 all-gather.10
  100.2 58.8 all-gather.8
  170.9 57.3 all-gather.12
where the time goes:
time: 242 us
  waiting for transfers between devices  143 us (59%)
  blocking collectives  28.3 us (12%)
  starting transfers between devices  23.7 us (10%)
  local copies, waits for them, and re-layouts  15.6 us (6%)
  between operations  13.3 us (5%)
  other arithmetic  10.6 us (4%)
  matrix products  7.26 us (3%)
    all_gather x2, waiting for transfers between devices, stacked_from(): parts = lax.all_gather(parts, axes[k])  65.5 us
    all_gather x1, waiting for transfers between devices, total_of_pieces(): parts = lax.all_gather(value, axis).astype(jnp.float32)  54 us
    all_gather x2, blocking collectives, stacked_from(): parts = lax.all_gather(parts, axes[k])  28.3 us
    all_to_all x2, starting transfers between devices, copy_for_each(): lax.all_to_all(jnp.broadcast_to(value[None], (length, *value.shape)), axi...  23.7 us
    all_to_all x2, waiting for transfers between devices, copy_for_each(): lax.all_to_all(jnp.broadcast_to(value[None], (length, *value.shape)), axi...  23.3 us
    transpose x2, local copies, waits for them, and re-layouts, stacked_from(): parts = parts.transpose(*back, *range(len(axes), parts.ndim))  9.76 us
    dot_general x1, matrix products, body(): jnp.dot(hidden, down_whole, preferred_element_type=jnp.float32) * down_scale  6.81 us
    reduce_sum x1, other arithmetic, total_of_pieces(): return parts.sum(axis=0)  5.41 us
  transfers between devices with their start and end apart: 5, of which 5 were waited for; matrix products, arithmetic and copies ran while one was open for 5% of the time, Pallas kernels for 0%

commit v1 on v0

v1 whole, which is shorter than its diff:
```python
import jax
import jax.numpy as jnp
from jax import lax
from jax.experimental import pallas as pl
from jax.experimental.pallas import tpu as pltpu
from jax.sharding import Mesh
from jax.sharding import PartitionSpec as P

MESH = pl.DeviceIdType.MESH
LENGTH = 128
NY, NZ, NX = 8, 4, 4
CUT = 32
EPS = 1e-06
F32, BF16 = jnp.float32, jnp.bfloat16
SIDES = (1, -1)
AROUND = (1, -1, 2)
SCHEDULE = (
    ("gy",), ("g", 0), ("start", 0), ("zo", 0), ("pool",), ("g", 1), ("g", 7), ("g", 2), ("g", 6), ("g", 3),
    ("g", 5), ("ay", 0, 1, 1), ("ay", 0, 1, -1), ("g", 4), ("zo", 1), ("by1", 0), ("ay", 0, 2, 1),
    ("ay", 0, 2, -1), ("mix",), ("by", 0, 1, 1, 0), ("azs", 0, -1), ("azs", 0, 1), ("azs", 0, -2),
    ("azs", 0, 2), ("by", 0, 1, -1, 0), ("by", 0, 1, 1, 1), ("by", 0, 1, -1, 1), ("ay", 0, 3, 1),
    ("azs", 0, -3), ("ay", 0, 3, -1), ("azs", 0, 3), ("by", 0, 2, 1, 0), ("cz",), ("cx", 0, 1), ("cx", 0, -1),
    ("by", 0, 2, -1, 0), ("by", 0, 2, 1, 1), ("start", 1), ("by", 0, 2, -1, 1), ("ay4", 0), ("azs", 0, 4),
    ("by", 0, 3, 1, 0), ("cx", 0, 2), ("by", 0, 3, -1, 0), ("by", 0, 3, 1, 1), ("by1", 1), ("norm", 0),
    ("ay", 1, 1, -1), ("azs", 1, 1), ("cx", 1, 1), ("cx", 1, -1), ("ay", 1, 1, 1), ("azs", 1, -1),
    ("by", 0, 3, -1, 1), ("by", 1, 1, -1, 0), ("by", 1, 1, 1, 0), ("cx", 1, 2), ("by", 1, 1, -1, 1),
    ("by", 1, 1, 1, 1), ("norm", 1), ("ay", 1, 2, -1), ("azs", 1, 2), ("ay", 1, 2, 1), ("azs", 1, -2),
    ("up",), ("by", 1, 2, 1, 0), ("by", 1, 2, -1, 0), ("comp", 0), ("by", 1, 2, 1, 1), ("by", 1, 2, -1, 1),
    ("ay", 1, 3, 1), ("azs", 1, -3), ("ay", 1, 3, -1), ("azs", 1, 3), ("comp", 1), ("rs1", 0),
    ("by", 1, 3, 1, 0), ("by", 1, 3, -1, 0), ("by", 1, 3, 1, 1), ("rs1", 1), ("by", 1, 3, -1, 1), ("ay4", 1),
    ("azs", 1, 4), ("comp", 2), ("rs2", 0), ("rs1", 2), ("rs2", 1), ("comp", 3), ("ag", 0), ("rs1", 3),
    ("om", 0), ("rs2", 2), ("ag", 1), ("om", 1), ("rs2", 3), ("ag", 2), ("om", 2), ("ag", 3), ("om", 3),
)

def message_keys():
    keys = [("Gy", d) for d in range(1, NY)] + [("Gz", d, e) for d in range(NY) for e in AROUND]
    keys += [("Cz",)] + [("Cx", j, d) for j in (0, 1) for d in AROUND]
    keys += [("Cm", j, d) for j in (0, 1) for d in (0, *AROUND)]
    for w in (0, 1):
        for s in SIDES:
            keys += [("Ay", w, k, s, part) for k in (1, 2, 3, 4) for part in (0, 1)]
            keys += [("By", w, k, s, h) for k in (1, 2, 3) for h in (0, 1)] + [("By", w, 4, s)]
            keys += [("Zo", w, s, n) for n in (1, 2)]
            keys += [("Az", w, o, s, n) for o in (1, -1, 2, -2, 3, -3, 4) for n in (1, 2)]
    for g in range(4):
        keys += [("Pm", g), ("Om", g)] + [("AG", g, d) for d in AROUND]
        keys += [("R", g, 0, d) for d in AROUND] + [("R", g, 1, d) for d in (0, *AROUND)]
    return {key: i for i, key in enumerate(keys)}


KEYS = message_keys()
SOURCES = [(0, d) for d in AROUND] + [(1, d) for d in (0, *AROUND)]


def kernel(
    tokens_hbm, mix_gain, group_hbm, group_scale, mlp_gain, up_hbm, up_scale, down_hbm, down_scale,
    out,
    tokens, group_w, up_w, down_w,
    gw, wu, wd, vu, vd, cx, xs, hidden, part, mate, summed, got, result, scale_at, pooled,
    ssem, rsem, lsem, osem,
):
    rep, z0, y0 = lax.axis_index("rep"), lax.axis_index("z"), lax.axis_index("y")
    x0, c0 = lax.axis_index("x"), lax.axis_index("core")
    tp = x0 * 2 + c0
    q = lax.rem(z0, 2)
    keep, relay = (wu, wd), (vu, vd)
    across = (((1,), (1,)), ((), ()))

    def y_at(d):
        return lax.rem(y0 + (d + NY), NY)

    def z_at(d):
        return lax.rem(z0 + (d + NZ), NZ)

    def x_at(d):
        return lax.rem(x0 + (d + NX), NX)

    def to_y(d):
        return {"y": y_at(d)}

    def to_z(d):
        line = lax.rem(rep * NZ + z0 + (d + 3 * NZ), 3 * NZ)
        return {"rep": lax.div(line, NZ), "z": lax.rem(line, NZ)}

    def to_x(d):
        return {"x": x_at(d)}

    def to_pair(d):
        pair = z0 + 1 - 2 * q
        return {"z": pair} if d == 0 else {"z": pair, "x": x_at(d)}

    to_mate = {"core": 1 - c0}
    sent = []

    def copy(key, ref, dst, device):
        i = KEYS[key]
        return pltpu.make_async_remote_copy(
            src_ref=ref,
            dst_ref=dst,
            send_sem=ssem.at[i],
            recv_sem=rsem.at[i],
            device_id=device,
            device_id_type=MESH,
        )

    def send(key, ref, device, dst=None):
        c = copy(key, ref, ref if dst is None else dst, device)
        c.start()
        sent.append(c)

    def arrived(key, ref):
        copy(key, ref, ref, to_mate).wait_recv()

    def aligned(start, size):
        return pl.ds(pl.multiple_of(start, size), size)

    peers = [to_y(d) for d in range(1, NY)] + [to_z(d) for d in (1, -1, 2, -2)]
    peers += [to_x(d) for d in AROUND] + [to_pair(d) for d in AROUND] + [to_mate]
    barrier = pltpu.get_barrier_semaphore()
    for peer in peers:
        pl.semaphore_signal(barrier, inc=1, device_id=peer, device_id_type=MESH)
    loads = [
        pltpu.make_async_copy(src, dst, lsem.at[i])
        for i, (src, dst) in enumerate(
            [(group_hbm, group_w), (up_hbm, up_w), (down_hbm, down_w), (tokens_hbm, tokens)]
        )
    ]
    for load in loads:
        load.start()

    def shard(w, o, dz, lo=0, hi=64):
        y = y_at(o)
        return keep[w].at[lax.div(y, 2), z_at(dz), lax.rem(y, 2), pl.ds(lo, hi - lo)]

    def b_half(w, o, h):
        y = y_at(o)
        return keep[w].at[lax.div(y, 2), pl.ds(2 * h, 2), lax.rem(y, 2), pl.ds(CUT, 64 - CUT)]

    def passed(w, o, lo=0, hi=64):
        return relay[w].at[y_at(o), pl.ds(lo, hi - lo)]

    def half(s, size, base=0):
        return (base, base + size // 2) if s == 1 else (base + size // 2, base + size)

    step = 1 - 2 * lax.rem(y0, 2)
    m0 = lax.div(y0, 2)
    pair_at = [lax.rem(m0 + d + 4, 4) for d in (0, -step, step, 2)]
    own_half = aligned(c0 * 128, 128)
    mate_half = aligned((1 - c0) * 128, 128)
    my_rows = aligned(c0 * 128 + x0 * 32, 32)

    def cast(w, src):
        mine, other = aligned(q * 512, 512), aligned((1 - q) * 512, 512)
        keep[w][m0, z0, lax.rem(y0, 2)] = src[:, mine].astype(BF16)
        relay[w][y0] = src[:, other].astype(BF16)

    def start(w):
        for s in SIDES:
            send(("Ay", w, 1, s, 0), shard(w, 0, 0, 0, CUT), to_y(s))
            send(("Ay", w, 1, s, 1), passed(w, 0, 0, CUT), to_y(s))

    def zo(w):
        for s in SIDES:
            send(("Zo", w, s, 1), passed(w, 0), to_z(s), shard(w, 0, 0))
        for s in SIDES:
            send(("Zo", w, s, 2), shard(w, 0, 0, *half(s, 64)), to_z(2 * s))

    def by1(w):
        for s in SIDES:
            arrived(("Zo", w, s, 1), shard(w, 0, -s))
            arrived(("Zo", w, s, 2), shard(w, 0, -2 * s, *half(s, 64)))
        for h in (0, 1):
            for s in SIDES:
                send(("By", w, 1, s, h), b_half(w, 0, h), to_y(s))

    def ay(w, k, s):
        arrived(("Ay", w, k, s, 0), shard(w, -s * k, 0, 0, CUT))
        arrived(("Ay", w, k, s, 1), passed(w, -s * k, 0, CUT))
        rows = (0, CUT) if k < 3 else half(s, CUT)
        send(("Ay", w, k + 1, s, 0), shard(w, -s * k, 0, *rows), to_y(s))
        send(("Ay", w, k + 1, s, 1), passed(w, -s * k, *rows), to_y(s))

    def ay4(w):
        for s in SIDES:
            arrived(("Ay", w, 4, s, 0), shard(w, 4, 0, *half(s, CUT)))
            arrived(("Ay", w, 4, s, 1), passed(w, 4, *half(s, CUT)))

    def azs(w, o):
        for s in SIDES:
            send(("Az", w, o, s, 1), passed(w, o, 0, CUT), to_z(s), shard(w, o, 0, 0, CUT))
            send(("Az", w, o, s, 2), shard(w, o, 0, *half(s, CUT)), to_z(2 * s))

    def by(w, k, s, h):
        arrived(("By", w, k, s, h), b_half(w, -s * k, h))
        if k < 3:
            send(("By", w, k + 1, s, h), b_half(w, -s * k, h), to_y(s))
        elif h == (0 if s == 1 else 1):
            send(("By", w, 4, s), b_half(w, -s * k, h), to_y(s))

    def complete(w, *slots):
        for o in slots:
            for s in SIDES:
                arrived(("Az", w, o, s, 1), shard(w, o, -s, 0, CUT))
                arrived(("Az", w, o, s, 2), shard(w, o, -2 * s, *half(s, CUT)))
                if o == 4:
                    arrived(("By", w, 4, s), b_half(w, 4, 0 if s == 1 else 1))

    width = tokens.shape[1]

    def gy():
        loads[0].wait()
        gw[z0, y0] = group_w[...].astype(BF16)
        loads[1].wait()
        cast(0, up_w)
        pl.semaphore_wait(barrier, len(peers))
        for d in (1, 7, 2, 6, 3, 5, 4):
            send(("Gy", d), gw.at[z0, y0], to_y(d))

    def g(d):
        if d:
            arrived(("Gy", d), gw.at[z0, y_at(-d)])
        for e in (1, -1, 2 if d % 2 == 0 else -2):
            send(("Gz", d, abs(e) if abs(e) == 2 else e), gw.at[z0, y_at(-d)], to_z(e))

    def pool():
        loads[2].wait()
        cast(1, down_w)
        loads[3].wait()
        own_group = aligned(x0 * 512, 512)
        whole = tokens[...].astype(F32)
        inverse = lax.rsqrt(jnp.sum(whole * whole, axis=-1, keepdims=True) / width + EPS)
        normed = (tokens[:, own_group].astype(F32) * inverse * mix_gain[:, own_group]).astype(BF16)
        row = lax.broadcasted_iota(jnp.int32, (LENGTH, LENGTH), 0)
        gap = row - lax.broadcasted_iota(jnp.int32, (LENGTH, LENGTH), 1)
        window = jnp.left_shift(jnp.int32(2), x0)
        band = ((gap >= 0) & (gap < window)).astype(F32).astype(BF16)
        position = lax.broadcasted_iota(jnp.int32, (LENGTH, 1), 0)
        divisor = jnp.minimum(position + 1, window).astype(F32)
        for n in range(tokens.shape[0] // LENGTH):
            piece = normed[n * LENGTH : (n + 1) * LENGTH]
            total = jnp.dot(band, piece, preferred_element_type=F32)
            pooled[n * LENGTH : (n + 1) * LENGTH] = (
                total / divisor - piece.astype(F32)
            ).astype(BF16)

    def mix():
        for d in range(NY):
            for e in AROUND:
                back = -e if e != 2 or d % 2 == 0 else 2
                arrived(("Gz", d, e), gw.at[z_at(back), y_at(-d)])
        mixed = jnp.dot(pooled[...], gw[...].reshape(512, 256), preferred_element_type=F32)
        own = tokens[:, aligned(tp * 256, 256)].astype(F32)
        cx[q, tp] = (own + mixed * group_scale[...]).astype(BF16)
        send(("Cz",), cx.at[q, tp], to_pair(0))
        for d in (2, 1, -1):
            send(("Cx", 0, d), cx.at[q, tp], to_x(d))
        send(("Cm", 0, 0), cx.at[q, tp], to_mate)

    def rows_of(j):
        return q if j == 0 else 1 - q

    def cz():
        arrived(("Cz",), cx.at[1 - q, tp])
        for d in (2, 1, -1):
            send(("Cx", 1, d), cx.at[1 - q, tp], to_x(d))
        send(("Cm", 1, 0), cx.at[1 - q, tp], to_mate)

    def cx_(j, d):
        block = cx.at[rows_of(j), x_at(-d) * 2 + c0]
        arrived(("Cx", j, d), block)
        send(("Cm", j, d), block, to_mate)

    def norm(j):
        for d in (0, *AROUND):
            arrived(("Cm", j, d), cx.at[rows_of(j), x_at(-d) * 2 + 1 - c0])
        at = rows_of(j)
        square = None
        for p in range(8):
            v = cx[at, p].astype(F32)
            s = jnp.sum(v * v, axis=-1, keepdims=True)
            square = s if square is None else square + s
        inverse = lax.rsqrt(square / width + EPS)
        for m in range(4):
            for z in range(NZ):
                v = cx[at, 2 * z + m // 2, :, (m % 2) * 128 : (m % 2) * 128 + 128].astype(F32)
                first = z * 512 + m * 128
                xs[m, at, :, z * 128 : z * 128 + 128] = (
                    v * inverse * mlp_gain[:, first : first + 128]
                ).astype(BF16)
        if j == 0:
            for m in range(4):
                for z in range(NZ):
                    first = z * 512 + m * 128
                    scale_at[m, :, z * 128 : z * 128 + 128] = down_scale[:, first : first + 128]

    def up():
        complete(0, 1, -1, 2, -2, 3, -3, 4)

        def tile(n, carry):
            cols = aligned(n * 256, 256)
            acc = None
            for m in range(4):
                t = jnp.dot(
                    xs[m].reshape(512, 512),
                    wu[m, :, :, :, cols].reshape(512, 256),
                    preferred_element_type=F32,
                )
                acc = t if acc is None else acc + t
            acc = jnp.maximum(acc * up_scale[:, aligned(q * 512 + n * 256, 256)], 0.0)
            hidden[:, cols] = (acc * acc).astype(BF16)
            return carry

        lax.fori_loop(0, 2, tile, 0)

    def comp(i):
        complete(1, *((1, -1), (2, -2), (3, -3), (4,))[i])
        m = pair_at[i]
        t = lax.dot_general(
            hidden[...], wd[m].reshape(512, 512), across, preferred_element_type=F32
        )
        part[i] = (t * scale_at[m]).astype(BF16).reshape(2, 256, 512)
        send(("Pm", i), part.at[i, :, mate_half], to_mate, mate.at[i])

    def rs1(i):
        arrived(("Pm", i), mate.at[i])
        summed[i] = (part[i, :, own_half].astype(F32) + mate[i].astype(F32)).astype(BF16)
        for d in (2, 1, -1, 0):
            rows = aligned(x_at(d) * 32, 32)
            place = got.at[i, SOURCES.index((1, d))]
            send(("R", i, 1, d), summed.at[i, 1 - q, rows], to_pair(d), place)
        for d in (2, 1, -1):
            rows = aligned(x_at(d) * 32, 32)
            place = got.at[i, SOURCES.index((0, d))]
            send(("R", i, 0, d), summed.at[i, q, rows], to_x(d), place)

    def rs2(i):
        m = pair_at[i]
        total = summed[i, q, aligned(x0 * 32, 32)].astype(F32)
        for n, (side, d) in enumerate(SOURCES):
            arrived(("R", i, side, d), got.at[i, n])
            total = total + got[i, n].astype(F32)
        for z in range(NZ):
            base = cx[q, 2 * z + lax.div(m, 2), my_rows, aligned(lax.rem(m, 2) * 128, 128)]
            lanes = slice(z * 128, z * 128 + 128)
            result[m, my_rows, lanes] = (base.astype(F32) + total[:, lanes]).astype(BF16)
        for d in (2, 1, -1):
            send(("AG", i, d), result.at[m, my_rows], to_x(d))

    def ag(i):
        m = pair_at[i]
        for d in AROUND:
            rows = aligned(c0 * 128 + x_at(-d) * 32, 32)
            arrived(("AG", i, d), result.at[m, rows])
        send(("Om", i), result.at[m, own_half], to_mate)

    stores = []

    def om(i):
        m = pair_at[i]
        arrived(("Om", i), result.at[m, mate_half])
        for z in range(NZ):
            c = pltpu.make_async_copy(
                result.at[m, :, pl.ds(z * 128, 128)],
                out.at[:, aligned(z * 512 + m * 128, 128)],
                osem.at[i, z],
            )
            c.start()
            stores.append(c)

    tasks = dict(
        gy=gy, g=g, start=start, zo=zo, by1=by1, ay=ay, ay4=ay4, azs=azs, by=by, pool=pool, mix=mix,
        cz=cz, cx=cx_, norm=norm, up=up, comp=comp, rs1=rs1, rs2=rs2, ag=ag, om=om,
    )
    for name, *where in SCHEDULE:
        with jax.named_scope("_".join([name, *(str(v) for v in where)])):
            tasks[name](*where)
    with jax.named_scope("stores"):
        for c in stores:
            c.wait()
    with jax.named_scope("sent"):
        for c in sent:
            c.wait_send()


def body(tokens, mix_gain, group_w, group_scale, mlp_gain, up_w, up_scale, down_w, down_scale):
    rows, width = tokens.shape
    n = len(KEYS)
    vmem, hbm = pl.BlockSpec(memory_space=pltpu.VMEM), pl.BlockSpec(memory_space=pl.ANY)
    shard_shape = up_w.shape
    return pl.pallas_call(
        kernel,
        name="layer",
        out_shape=jax.ShapeDtypeStruct((rows, width), BF16),
        in_specs=[hbm, vmem, hbm, vmem, vmem, hbm, vmem, hbm, vmem],
        out_specs=hbm,
        scratch_shapes=[
            pltpu.VMEM((rows, width), BF16),
            pltpu.VMEM(group_w.shape, F32),
            pltpu.VMEM(shard_shape, F32),
            pltpu.VMEM(shard_shape, F32),
            pltpu.VMEM((NZ, NY, 16, 256), BF16),
            pltpu.VMEM((4, NZ, 2, 64, 512), BF16),
            pltpu.VMEM((4, NZ, 2, 64, 512), BF16),
            pltpu.VMEM((NY, 64, 512), BF16),
            pltpu.VMEM((NY, 64, 512), BF16),
            pltpu.VMEM((2, 8, rows, 256), BF16),
            pltpu.VMEM((4, 2, rows, 512), BF16),
            pltpu.VMEM((2 * rows, 512), BF16),
            pltpu.VMEM((4, 2, rows, 512), BF16),
            pltpu.VMEM((4, 2, rows // 2, 512), BF16),
            pltpu.VMEM((4, 2, rows // 2, 512), BF16),
            pltpu.VMEM((4, len(SOURCES), 32, 512), BF16),
            pltpu.VMEM((4, rows, 512), BF16),
            pltpu.VMEM((4, 1, 512), F32),
            pltpu.VMEM((rows, 512), BF16),
            pltpu.SemaphoreType.DMA((n,)),
            pltpu.SemaphoreType.DMA((n,)),
            pltpu.SemaphoreType.DMA((4,)),
            pltpu.SemaphoreType.DMA((4, NZ)),
        ],
        compiler_params=pltpu.CompilerParams(
            collective_id=0, has_side_effects=True, vmem_limit_bytes=56 * 1024 * 1024
        ),
    )(
        tokens,
        mix_gain.reshape(1, width),
        group_w,
        group_scale,
        mlp_gain.reshape(1, width),
        up_w,
        up_scale,
        down_w.T,
        down_scale,
    )


def solution(mesh):
    split = Mesh(
        mesh.devices.reshape(mesh.shape["rep"], NZ, NY, NX, 2), ("rep", "z", "y", "x", "core")
    )
    fs, tp = ("z", "y"), ("x", "core")
    rows = P(("rep", "z", "y"), None)
    return jax.shard_map(
        body,
        mesh=split,
        in_specs=(
            rows,
            P(),
            P(fs, tp),
            P(None, tp),
            P(),
            P(fs, tp),
            P(None, tp),
            P(tp, fs),
            P(),
        ),
        out_specs=rows,
        check_vma=False,
    )
```

time: 242 us -> 85.4 us (0.35)
  waiting for transfers between devices: 143 us -> 0 us
  Pallas kernels: 0 us -> 82.8 us
  blocking collectives: 28.3 us -> 0 us
  starting transfers between devices: 23.7 us -> 0 us
  local copies, waits for them, and re-layouts: 15.6 us -> 2.3 us
  between operations: 13.3 us -> 0.01 us
  other arithmetic: 10.6 us -> 0 us
  matrix products: 7.26 us -> 0 us
    all_gather x3 -> x0, waiting for transfers between devices: 120 us -> none  [the longest x2 65.5 us: stacked_from(): parts = lax.all_gather(parts, axes[k])]
    pallas_call x0 -> x1, Pallas kernels: none -> 82.8 us  [body(): pl.pallas_call(kernel, name='layer', out_shape=jax.ShapeDtypeStruct((rows...]
    all_gather x2 -> x0, blocking collectives: 28.3 us -> none  [stacked_from(): parts = lax.all_gather(parts, axes[k])]
    all_to_all x2 -> x0, starting transfers between devices: 23.7 us -> none  [copy_for_each(): lax.all_to_all(jnp.broadcast_to(value[None], (length, *value.shape)), axi...]
    all_to_all x2 -> x0, waiting for transfers between devices: 23.3 us -> none  [copy_for_each(): lax.all_to_all(jnp.broadcast_to(value[None], (length, *value.shape)), axi...]
    transpose x2 -> x0, local copies, waits for them, and re-layouts: 9.76 us -> none  [stacked_from(): parts = parts.transpose(*back, *range(len(axes), parts.ndim))]
    dot_general x3 -> x0, matrix products: 7.26 us -> none  [the longest x1 6.81 us: body(): jnp.dot(hidden, down_whole, preferred_element_type=jnp.float32) * down_scale]
    reduce_sum x3 -> x0, other arithmetic: 6 us -> none  [the longest x1 5.41 us: total_of_pieces(): return parts.sum(axis=0)]
  transfers between devices with their start and end apart: 5 -> 0, of which waited for: 5 -> 0; matrix products, arithmetic and copies ran while one was open for 5% -> 0% of each run, Pallas kernels for 0% -> 0%
where the time goes in v1:
time: 85.4 us; the launch traced here: 85.1 us
  Pallas kernels  82.8 us (97%)
  local copies, waits for them, and re-layouts  2.3 us (3%)
    pallas_call x1, Pallas kernels, body(): pl.pallas_call(kernel, name='layer', out_shape=jax.ShapeDtypeStruct((rows...  82.8 us
    unnamed x1, local copies, waits for them, and re-layouts  2.3 us

profile of v1, /device:TPU:1, one launch (start us, length us, event | category | flops | bytes accessed | tf_op | source)
XLA Modules:
  0.0 85.1 jit_solution(12691168956047504493)
XLA Ops:
  0.0 82.8 %layer.1 = bf16[256,2048]{1,0:T(8,128)(2,1)} custom-call(bf16[256,2048]{1,0:T(8,128)(2,1)} %tokens_hbm.1, f32[1,2048]{1,0:T(1,128)} %bitcast.4, f32[16,256]{1,0:T(8,128)} %group_hbm.1, f32[1,256]{1,0:T(1,128)} %group_scale.1, f32[1,2048]{1,0:T(1,128)} %bitcast.5, f32[64,1024]{1,0:T(8,128)} %up_hbm.1, f32[1,1024]{1,0:T(1,128)} %up_scale.1, ...), custom_call_target="tpu_custom_call" | custom-call | tf_op jit(solution)/shard_map/layer/pallas_call | solution.py:390
  82.8 2.3 %copy.11 = bf16[256,2048]{1,0:T(8,128)(2,1)} copy(bf16[256,2048]{1,0:T(8,128)(2,1)} %layer.1) | data formatting | bytes 2097152
